TPU v7x, 32 devices: a whole 2x2x4 slice. The times are simulated.
32 devices in a mesh: grp: 2 (over x), ep: 16 (over z, y, core).
Axes of the slice: x: 2, y: 2, z: 4, core: 2. Of those that a mesh axis runs over, the one named last changes fastest.
Arguments:
- residual: bfloat16 [16, 4096], P('grp', 'ep'), parts along dimension 0, may hold values from -6 to 6
- head_states: float32 [64, 512, 1024], P(('grp', 'ep')), parts along dimension 0, may hold values from -6 to 6
- first_gain: bfloat16 [4096], replicated, may hold values from 0.099609375 to 1.8984375
- w_query: bfloat16 [4096, 2048], P(None, 'ep'), may hold values from -0.09375 to 0.09375
- w_key: bfloat16 [4096, 2048], P(None, 'ep'), may hold values from -0.09375 to 0.09375
- w_value: bfloat16 [4096, 4096], P(None, 'ep'), may hold values from -0.09375 to 0.09375
- w_gate: bfloat16 [4096, 4096], P(None, 'ep'), may hold values from -0.09375 to 0.09375
- w_low: bfloat16 [4096, 16], replicated, may hold values from -0.09375 to 0.09375
- w_decay: bfloat16 [16, 2048], replicated, may hold values from -15 to 15
- decay_bias: float32 [2048], replicated, may hold values from -40 to 4
- head_gain: bfloat16 [1024], replicated, may hold values from 0.099609375 to 1.8984375
- w_output: bfloat16 [4096, 4096], P(None, 'ep'), may hold values from -0.09375 to 0.09375
- second_gain: bfloat16 [4096], replicated, may hold values from 0.099609375 to 1.8984375
- routes: int32 [16, 2], P('grp'), parts along dimension 0, may hold values from 0 to 15, as said below
- group_logits: float32 [16, 4], P('grp'), parts along dimension 0, may hold values from -12 to 12
- expert_logits: float32 [16, 2], P('grp'), parts along dimension 0, may hold values from -9 to 9
- expert_gate: bfloat16 [16, 4096, 512], P('ep'), may hold values from -0.09375 to 0.09375
- expert_up: bfloat16 [16, 4096, 512], P('ep'), may hold values from -0.09375 to 0.09375
- expert_down: bfloat16 [16, 512, 4096], P('ep'), may hold values from -0.25 to 0.25
Outputs:
- layer_out: bfloat16 [16, 4096], P('grp', 'ep'), parts along dimension 0
- new_states: float32 [64, 512, 1024], P(('grp', 'ep')), parts along dimension 0
There are 2 independent parts, one for each index of `grp`. A program takes and returns all parts, laid end to end along the dimension named above; an argument that names none is the same for every part. Nothing has to cross between parts.
Inputs may be any that keep to these rules, and one draw needn't show every extreme that they name: `routes`: each row names 2 different experts of one group (numbers g * 4 to g * 4 + 3). No expert is named by more than 2 rows, and in every draw all experts of one group are named by exactly 2 rows.
All inputs are finite; a program needn't handle non-finite values.
Results may differ from a plain program's by a relative error of at most 0.014.
Values may be sent and summed in bfloat16 or wider, within the bound.
No kernel may reach another device: no remote copies, remote signals or barrier semaphores. Data moves between devices by JAX's collectives and lax.ppermute only.
A program may use at most 128 MiB of HBM per device.

v0:
```python
import jax
import jax.numpy as jnp
import numpy as np
from jax import lax
from jax.sharding import PartitionSpec as P

HEADS = 4
DK = 512
DV = 1024
GROUPS = 4
TOP = 2
norm_eps = 1e-06
decay_tau = 16.0


def rms_scale(values, gain):
    floats = values.astype(jnp.float32)
    return (
        floats
        * lax.rsqrt(jnp.mean(floats * floats, axis=-1, keepdims=True) + norm_eps)
        * gain.astype(jnp.float32)
    )


def route_weights(routes, group_logits, expert_logits, per_group):
    group_exp = jnp.exp(group_logits)
    group_prob = group_exp / jnp.sum(group_exp, axis=1, keepdims=True)
    chosen = routes[:, 0] // per_group
    groups_row = jnp.arange(group_logits.shape[1], dtype=jnp.int32)
    picked = jnp.sum(
        group_prob * (chosen[:, None] == groups_row[None, :]).astype(jnp.float32), axis=1
    )
    expert_exp = jnp.exp(expert_logits)
    return expert_exp / jnp.sum(expert_exp, axis=1, keepdims=True) * picked[:, None]


def per_device(
    residual,
    head_states,
    first_gain,
    w_query,
    w_key,
    w_value,
    w_gate,
    w_low,
    w_decay,
    decay_bias,
    head_gain,
    w_output,
    second_gain,
    routes,
    group_logits,
    expert_logits,
    expert_gate,
    expert_up,
    expert_down,
):
    devices = lax.axis_size("ep")
    my_index = lax.axis_index("ep")
    seq_count = residual.shape[0]
    own_width = residual.shape[1]
    width = own_width * devices
    pairs_dev = head_states.shape[0]
    slot_count = max(1, pairs_dev // HEADS)
    rows = lax.all_gather(residual, "ep", axis=1, tiled=True)
    normed = rms_scale(rows, first_gain).astype(jnp.bfloat16)
    my_head = my_index * HEADS // devices
    target = jnp.arange(devices, dtype=jnp.int32)[:, None]
    turn = jnp.arange(slot_count, dtype=jnp.int32)[None, :]
    within = jnp.mod(my_head - target * pairs_dev, HEADS) + turn * HEADS
    target_seq = (target * pairs_dev + within) // HEADS
    seq_row = jnp.arange(seq_count, dtype=jnp.int32)[None, None, :]
    picker = (target_seq[:, :, None] == seq_row) & (within < pairs_dev)[:, :, None]
    picker = picker.astype(jnp.bfloat16).reshape(devices * slot_count, seq_count)

    def outgoing(weight):
        projected = jnp.dot(normed, weight, preferred_element_type=jnp.float32).astype(jnp.bfloat16)
        placed = jnp.dot(picker, projected, preferred_element_type=jnp.float32).astype(jnp.bfloat16)
        return placed.reshape(devices, slot_count, projected.shape[1])

    send_query = outgoing(w_query)
    send_key = outgoing(w_key)
    send_value = outgoing(w_value)
    send_gate = outgoing(w_gate)
    incoming = (
        lax.all_to_all(send_query, "ep", split_axis=0, concat_axis=0, tiled=True),
        lax.all_to_all(send_key, "ep", split_axis=0, concat_axis=0, tiled=True),
        lax.all_to_all(send_value, "ep", split_axis=0, concat_axis=0, tiled=True),
        lax.all_to_all(send_gate, "ep", split_axis=0, concat_axis=0, tiled=True),
    )
    pair_ids = my_index * pairs_dev + jnp.arange(pairs_dev, dtype=jnp.int32)
    head_pick = (
        jnp.mod(pair_ids, HEADS)[:, None] == jnp.arange(HEADS, dtype=jnp.int32)[None, :]
    ).astype(jnp.bfloat16)
    turns = np.arange(pairs_dev) // HEADS
    pair_rows = np.arange(pairs_dev)

    def arrange(received):
        merged = jnp.dot(head_pick, received.reshape(HEADS, -1), preferred_element_type=jnp.float32)
        merged = merged.reshape(pairs_dev, devices // HEADS, slot_count, received.shape[2])
        return merged[pair_rows, :, turns, :].reshape(pairs_dev, -1).astype(jnp.bfloat16)

    query = arrange(incoming[0])
    key = arrange(incoming[1])
    value = arrange(incoming[2])
    gate = arrange(incoming[3])
    low = jnp.dot(normed, w_low, preferred_element_type=jnp.float32)
    decay_pre = (
        jnp.dot(low, w_decay.astype(jnp.float32), precision=lax.Precision.HIGHEST) + decay_bias
    )
    decay_pre = lax.dynamic_slice_in_dim(
        decay_pre.reshape(seq_count * HEADS, DK), my_index * pairs_dev, pairs_dev, 0
    )
    log_decay = jax.nn.log_sigmoid(decay_pre) / decay_tau
    new_states = (
        head_states * jnp.exp(log_decay)[:, :, None]
        + key.astype(jnp.float32)[:, :, None] * value.astype(jnp.float32)[:, None, :]
    )
    read = jnp.einsum(
        "pk,pkv->pv",
        query.astype(jnp.float32) * DK ** (-0.5),
        new_states,
        precision=lax.Precision.HIGHEST,
    )
    mixed = (rms_scale(read, head_gain) * jax.nn.silu(gate.astype(jnp.float32))).astype(
        jnp.bfloat16
    )
    gathered = lax.all_gather(mixed, "ep", axis=0, tiled=True).reshape(seq_count, HEADS * DV)
    branch = jnp.dot(gathered, w_output, preferred_element_type=jnp.float32).astype(jnp.bfloat16)
    stream = (residual.astype(jnp.float32) + branch.astype(jnp.float32)).astype(jnp.bfloat16)
    floats = stream.astype(jnp.float32)
    total = lax.psum(jnp.sum(floats * floats, axis=1), "ep")
    gain_part = lax.dynamic_slice_in_dim(second_gain, my_index * own_width, own_width)
    scaled = floats * lax.rsqrt(total / width + norm_eps)[:, None] * gain_part.astype(jnp.float32)
    expert_in = lax.all_gather(scaled.astype(jnp.bfloat16), "ep", axis=1, tiled=True)
    capacity = 2 * seq_count * TOP // devices
    weights = route_weights(routes, group_logits, expert_logits, devices // GROUPS)
    hits = (routes == my_index).astype(jnp.int32)
    mine = jnp.sum(weights * hits.astype(jnp.float32), axis=1)
    routed = jnp.sum(hits, axis=1)
    slot = jnp.cumsum(routed) - routed
    chooser = (slot[None, :] == jnp.arange(capacity, dtype=jnp.int32)[:, None]) & (
        routed[None, :] > 0
    )
    picked = jnp.dot(
        chooser.astype(jnp.bfloat16), expert_in, preferred_element_type=jnp.float32
    ).astype(jnp.bfloat16)
    row_weight = jnp.dot(chooser.astype(jnp.float32), mine, precision=lax.Precision.HIGHEST)
    gate_part = jnp.dot(picked, expert_gate[0], preferred_element_type=jnp.float32)
    up_part = jnp.dot(picked, expert_up[0], preferred_element_type=jnp.float32)
    active = (jax.nn.silu(gate_part) * up_part * row_weight[:, None]).astype(jnp.bfloat16)
    expert_rows = jnp.dot(active, expert_down[0], preferred_element_type=jnp.float32).astype(
        jnp.bfloat16
    )
    arrived = lax.all_to_all(expert_rows, "ep", split_axis=1, concat_axis=0, tiled=True)
    every = jnp.arange(devices, dtype=jnp.int32)
    hit_all = jnp.sum((routes[:, :, None] == every[None, None, :]).astype(jnp.int32), axis=1)
    slot_all = jnp.cumsum(hit_all, axis=0) - hit_all
    placer = (slot_all[:, :, None] == jnp.arange(capacity, dtype=jnp.int32)[None, None, :]) & (
        hit_all[:, :, None] > 0
    )
    placer = placer.astype(jnp.bfloat16).reshape(seq_count, devices * capacity)
    returned = jnp.dot(placer, arrived, preferred_element_type=jnp.float32)
    layer_out = (stream.astype(jnp.float32) + returned).astype(jnp.bfloat16)
    return (layer_out, new_states)


def solution(mesh):
    return jax.shard_map(
        per_device,
        mesh=mesh,
        in_specs=(
            P("grp", "ep"),
            P(("grp", "ep"), None, None),
            P(),
            P(None, "ep"),
            P(None, "ep"),
            P(None, "ep"),
            P(None, "ep"),
            P(),
            P(),
            P(),
            P(),
            P(None, "ep"),
            P(),
            P("grp", None),
            P("grp", None),
            P("grp", None),
            P("ep", None, None),
            P("ep", None, None),
            P("ep", None, None),
        ),
        out_specs=(P("grp", "ep"), P(("grp", "ep"), None, None)),
        check_vma=False,
    )
```

profile of v0, /device:TPU:0, one launch (start us, length us, event | category | flops | bytes accessed | tf_op | source)
XLA Modules:
  0.0 169.2 jit_solution(12246803465482614124)
XLA Ops:
  0.7 23.7 %all_gather.9 = bf16[8,4096]{1,0:T(8,128)(2,1)S(1)} all-gather(bf16[8,256]{1,0:T(8,128)(2,1)} %param.29), channel_id=1, replica_groups=mesh['grp'=2,'ep'=16] {'ep'}, dimensions={1}, use_global_device_ids=true | all-gather | bytes 69632 | tf_op jit(solution)/shard_map/all_gather | solution.py:65
  24.6 0.7 convert_element_type.145
  25.3 1.6 fusion.14
  26.9 0.6 copy.61
  27.5 3.4 %all-to-all-start.1 = ((bf16[16,1,128]{2,1,0:T(2,128)(2,1)}), bf16[16,1,128]{2,1,0:T(2,128)(2,1)S(1)}, u32[]{:S(2)}, u32[]{:S(2)}) async-start(bf16[16,1,128]{2,1,0:T(2,128)(2,1)} %copy.61), calls=%async_computation.1 | async-start | bytes 16384 | tf_op jit(solution)/shard_map/all_to_all | solution.py:87
  31.0 0.7 fusion.70
  31.7 0.7 fusion.73
  32.4 0.8 convert_reduce_fusion
  33.6 1.1 fusion.88
  34.8 1.0 convolution_add_fusion
  35.8 1.6 fusion.13
  37.4 2.1 %fusion.6 = bf16[16,1,256]{2,0,1:T(8,128)(2,1)S(1)} fusion(bf16[4096,256]{1,0:T(8,128)(2,1)} %param.35, s32[16]{0:T(128)S(1)} %and_select_fusion.1, pred[16]{0:T(512)(128)(4,1)S(1)} %broadcast_compare_fusion.2, bf16[8,4096]{1,0:T(8,128)(2,1)S(1)} %all_gather.9, f32[4096]{0:T(1024)S(1)} %convert_element_type.145, f32[8]{0:T(128)S(1)} %add_rsqrt_fusion.2), kind=kOutput, calls=%fused_computation.16 | convolution fusion | flops 16980224 | bytes 2187376 | tf_op jit(solution)/shard_map/dot_general | solution.py:78
  39.9 0.8 dynamic-slice_convert_fusion
  41.3 0.6 reduce.5
  43.2 0.6 reduce.4
  44.5 6.0 %all-to-all-start = ((bf16[16,1,128]{2,1,0:T(2,128)(2,1)}), bf16[16,1,128]{2,1,0:T(2,128)(2,1)S(1)}, u32[]{:S(2)}, u32[]{:S(2)}) async-start(bf16[16,1,128]{2,1,0:T(2,128)(2,1)} %copy.59), calls=%async_computation | async-start | bytes 16384 | tf_op jit(solution)/shard_map/all_to_all | solution.py:86
  51.3 5.5 %all-to-all-done = bf16[16,1,128]{2,1,0:T(2,128)(2,1)S(1)} async-done(((bf16[16,1,128]{2,1,0:T(2,128)(2,1)}), bf16[16,1,128]{2,1,0:T(2,128)(2,1)S(1)}, u32[]{:S(2)}, u32[]{:S(2)}) %all-to-all-start) | async-done | bytes 4128 | tf_op jit(solution)/shard_map/all_to_all | solution.py:86
  56.8 3.4 %all-to-all-start.2 = ((bf16[16,2,128]{2,1,0:T(2,128)(2,1)}), bf16[16,2,128]{2,1,0:T(2,128)(2,1)S(1)}, u32[]{:S(2)}, u32[]{:S(2)}) async-start(bf16[16,2,128]{2,1,0:T(2,128)(2,1)} %reshape.330), calls=%async_computation.2 | async-start | bytes 16384 | tf_op jit(solution)/shard_map/all_to_all | solution.py:88
  61.1 5.6 %all-to-all-done.2 = bf16[16,2,128]{2,1,0:T(2,128)(2,1)S(1)} async-done(((bf16[16,2,128]{2,1,0:T(2,128)(2,1)}), bf16[16,2,128]{2,1,0:T(2,128)(2,1)S(1)}, u32[]{:S(2)}, u32[]{:S(2)}) %all-to-all-start.2) | async-done | bytes 8224 | tf_op jit(solution)/shard_map/all_to_all | solution.py:88
  66.6 3.5 %all-to-all-start.3 = ((bf16[16,2,128]{2,1,0:T(2,128)(2,1)}), bf16[16,2,128]{2,1,0:T(2,128)(2,1)S(1)}, u32[]{:S(2)}, u32[]{:S(2)}) async-start(bf16[16,2,128]{2,1,0:T(2,128)(2,1)} %reshape.328), calls=%async_computation.3 | async-start | bytes 16384 | tf_op jit(solution)/shard_map/all_to_all | solution.py:89
  71.0 2.7 %multiply_add_fusion = f32[2,512,1024]{2,1,0:T(8,128)S(1)} fusion(f32[2,512,1024]{2,1,0:T(8,128)} %param.30, f32[2,1024]{1,0:T(2,128)S(1)} %bitcast.122, f32[2,512]{1,0:T(2,128)S(1)} %bitcast.124, f32[2,512]{1,0:T(2,128)S(1)} %fusion.44), kind=kLoop, calls=%fused_computation.11 | loop fusion | flops 3145728 | bytes 8404992 | tf_op jit(solution)/shard_map/add | solution.py:116
  73.8 2.0 %copy-done.1 = f32[2,512,1024]{2,1,0:T(8,128)} copy-done((f32[2,512,1024]{2,1,0:T(8,128)}, f32[2,512,1024]{2,1,0:T(8,128)S(1)}, u32[]{:S(2)}) %copy-start.1) | copy-done | bytes 4194328
  75.8 2.1 %fusion.92 = f32[2,1,1024]{2,1,0:T(1,128)S(1)} fusion(f32[2,512,1]{1,2,0:T(1,128)S(1)} %bitcast.123, f32[2,512,1024]{2,1,0:T(8,128)S(1)} %multiply_add_fusion), kind=kOutput, calls=%fused_computation.142 | convolution fusion | flops 12582912 | bytes 4206592 | tf_op jit(solution)/shard_map/pk,pkv->pv/dot_general | solution.py:119
  78.9 21.8 %all-gather = bf16[16,2,1024]{2,1,0:T(2,128)(2,1)S(1)} all-gather(bf16[1,2,1024]{2,1,0:T(2,128)(2,1)S(1)} %fusion.60), channel_id=1, replica_groups=mesh['grp'=2,'ep'=16] {'ep'}, dimensions={0}, use_global_device_ids=true | all-gather | bytes 69632 | tf_op jit(solution)/shard_map/all_gather | solution.py:128
  100.8 2.1 %multiply_reduce_fusion = (f32[8]{0:T(128)S(1)}, f32[8,256]{1,0:T(8,128)S(1)}) fusion(bf16[8,4096]{1,0:T(8,128)(2,1)S(1)} %reshape.284, bf16[4096,256]{1,0:T(8,128)(2,1)} %param.40, bf16[8,256]{1,0:T(8,128)(2,1)S(1)} %copy-done.2), kind=kOutput, calls=%fused_computation.58 | convolution fusion | flops 16793592 | bytes 2175008 | tf_op jit(solution)/shard_map/dot_general | solution.py:129
  102.9 29.8 %psum.7 = f32[8]{0:T(128)S(1)} all-reduce(f32[8]{0:T(128)S(1)} %get-tuple-element.2), channel_id=1, replica_groups=mesh['grp'=2,'ep'=16] {'ep'}, use_global_device_ids=true, to_apply=%region_7.8 | all-reduce | flops 8 | bytes 64 | tf_op jit(solution)/shard_map/psum | solution.py:132
  132.8 17.3 %all_gather.11 = bf16[8,4096]{1,0:T(8,128)(2,1)S(1)} all-gather(bf16[8,256]{1,0:T(8,128)(2,1)S(1)} %multiply_convert_fusion), channel_id=1, replica_groups=mesh['grp'=2,'ep'=16] {'ep'}, dimensions={1}, use_global_device_ids=true | all-gather | bytes 69632 | tf_op jit(solution)/shard_map/all_gather | solution.py:135
  150.2 2.8 %fusion.3 = f32[2,512]{1,0:T(2,128)S(1)} fusion(bf16[2,4096]{1,0:T(2,128)(2,1)S(1)} %convolution_convert_fusion.1, bf16[1,4096,512]{2,1,0:T(8,128)(2,1)} %param.45), kind=kOutput, calls=%fused_computation.9 | convolution fusion | flops 8388608 | bytes 4214784 | tf_op jit(solution)/shard_map/dot_general | solution.py:149
  153.1 5.4 %convolution_convert_fusion = bf16[2,4096]{1,0:T(2,128)(2,1)} fusion(bf16[1,512,4096]{2,1,0:T(8,128)(2,1)} %param.47, bf16[2,4096]{1,0:T(2,128)(2,1)S(1)} %convolution_convert_fusion.1, bf16[1,4096,512]{2,1,0:T(8,128)(2,1)} %param.46, f32[2,512]{1,0:T(2,128)S(1)} %fusion.3, f32[2]{0:T(128)S(1)} %convolution_bitcast_fusion.5), kind=kOutput, calls=%fused_computation.4 | convolution fusion | flops 16792576 | bytes 8425480 | tf_op jit(solution)/shard_map/dot_general | solution.py:152
  158.4 3.5 %all-to-all-start.4 = ((bf16[2,16,256]{2,0,1:T(2,128)(2,1)}), bf16[2,16,256]{2,0,1:T(2,128)(2,1)S(1)}, u32[]{:S(2)}, u32[]{:S(2)}) async-start(bf16[2,16,256]{2,0,1:T(2,128)(2,1)} %bitcast.28), calls=%async_computation.4 | async-start | bytes 32768 | tf_op jit(solution)/shard_map/all_to_all | solution.py:155
  162.0 6.4 %all-to-all-done.4 = bf16[2,16,256]{2,0,1:T(2,128)(2,1)S(1)} async-done(((bf16[2,16,256]{2,0,1:T(2,128)(2,1)}), bf16[2,16,256]{2,0,1:T(2,128)(2,1)S(1)}, u32[]{:S(2)}, u32[]{:S(2)}) %all-to-all-start.4) | async-done | bytes 16416 | tf_op jit(solution)/shard_map/all_to_all | solution.py:155
  168.4 0.8 fusion.8
  (76 shorter events, 7.4 us)
Async XLA Ops:
  0.6 32.5 %copy-start = (bf16[4096,256]{1,0:T(8,128)(2,1)S(1)}, bf16[4096,256]{1,0:T(8,128)(2,1)}, u32[]{:S(2)}) copy-start(bf16[4096,256]{1,0:T(8,128)(2,1)} %param.34) | copy-start | bytes 6291460
  0.6 40.0 %copy-start.3 = (s32[8,2]{0,1:T(2,128)S(1)}, s32[8,2]{0,1:T(2,128)}, u32[]{:S(2)}) copy-start(s32[8,2]{0,1:T(2,128)} %param.42) | copy-start | bytes 196
  0.7 39.1 %copy-start.4 = (f32[8,4]{0,1:T(4,128)S(1)}, f32[8,4]{0,1:T(4,128)}, u32[]{:S(2)}) copy-start(f32[8,4]{0,1:T(4,128)} %param.43) | copy-start | bytes 388
  0.7 39.1 %copy-start.6 = (f32[8,2]{0,1:T(2,128)S(1)}, f32[8,2]{0,1:T(2,128)}, u32[]{:S(2)}) copy-start(f32[8,2]{0,1:T(2,128)} %param.44) | copy-start | bytes 196
  0.7 43.8 %copy-start.5 = (bf16[1024]{0:T(1024)(128)(2,1)S(1)}, bf16[1024]{0:T(1024)(128)(2,1)}, u32[]{:S(2)}) copy-start(bf16[1024]{0:T(1024)(128)(2,1)} %param.39) | copy-start | bytes 6148
  27.5 16.9 %all-to-all-start.1 = ((bf16[16,1,128]{2,1,0:T(2,128)(2,1)}), bf16[16,1,128]{2,1,0:T(2,128)(2,1)S(1)}, u32[]{:S(2)}, u32[]{:S(2)}) async-start(bf16[16,1,128]{2,1,0:T(2,128)(2,1)} %copy.61), calls=%async_computation.1 | async-start | bytes 16384 | tf_op jit(solution)/shard_map/all_to_all | solution.py:87
  44.5 12.3 %all-to-all-start = ((bf16[16,1,128]{2,1,0:T(2,128)(2,1)}), bf16[16,1,128]{2,1,0:T(2,128)(2,1)S(1)}, u32[]{:S(2)}, u32[]{:S(2)}) async-start(bf16[16,1,128]{2,1,0:T(2,128)(2,1)} %copy.59), calls=%async_computation | async-start | bytes 16384 | tf_op jit(solution)/shard_map/all_to_all | solution.py:86
  56.8 9.8 %all-to-all-start.2 = ((bf16[16,2,128]{2,1,0:T(2,128)(2,1)}), bf16[16,2,128]{2,1,0:T(2,128)(2,1)S(1)}, u32[]{:S(2)}, u32[]{:S(2)}) async-start(bf16[16,2,128]{2,1,0:T(2,128)(2,1)} %reshape.330), calls=%async_computation.2 | async-start | bytes 16384 | tf_op jit(solution)/shard_map/all_to_all | solution.py:88
  66.6 11.3 %all-to-all-start.3 = ((bf16[16,2,128]{2,1,0:T(2,128)(2,1)}), bf16[16,2,128]{2,1,0:T(2,128)(2,1)S(1)}, u32[]{:S(2)}, u32[]{:S(2)}) async-start(bf16[16,2,128]{2,1,0:T(2,128)(2,1)} %reshape.328), calls=%async_computation.3 | async-start | bytes 16384 | tf_op jit(solution)/shard_map/all_to_all | solution.py:89
  73.7 2.0 %copy-start.1 = (f32[2,512,1024]{2,1,0:T(8,128)}, f32[2,512,1024]{2,1,0:T(8,128)S(1)}, u32[]{:S(2)}) copy-start(f32[2,512,1024]{2,1,0:T(8,128)S(1)} %multiply_add_fusion) | copy-start | bytes 12582916
  73.8 27.0 %copy-start.2 = (bf16[8,256]{1,0:T(8,128)(2,1)S(1)}, bf16[8,256]{1,0:T(8,128)(2,1)}, u32[]{:S(2)}) copy-start(bf16[8,256]{1,0:T(8,128)(2,1)} %param.29) | copy-start | bytes 12292
  158.4 10.0 %all-to-all-start.4 = ((bf16[2,16,256]{2,0,1:T(2,128)(2,1)}), bf16[2,16,256]{2,0,1:T(2,128)(2,1)S(1)}, u32[]{:S(2)}, u32[]{:S(2)}) async-start(bf16[2,16,256]{2,0,1:T(2,128)(2,1)} %bitcast.28), calls=%async_computation.4 | async-start | bytes 32768 | tf_op jit(solution)/shard_map/all_to_all | solution.py:155
where the time goes:
time: 170 us; the launch traced here: 169 us
  blocking collectives  92.6 us (54%)
  matrix products  22.2 us (13%)
  starting transfers between devices  19.8 us (12%)
  waiting for transfers between devices  17.5 us (10%)
  other arithmetic  8.69 us (5%)
  local copies, waits for them, and re-layouts  7.43 us (4%)
    psum x1, blocking collectives, per_device(): total = lax.psum(jnp.sum(floats * floats, axis=1), 'ep')  29.8 us
    all_gather x1, blocking collectives, per_device(): rows = lax.all_gather(residual, 'ep', axis=1, tiled=True)  23.7 us
    all_gather x1, blocking collectives, per_device(): lax.all_gather(mixed, 'ep', axis=0, tiled=True)  21.8 us
    all_gather x1, blocking collectives, per_device(): lax.all_gather(scaled.astype(jnp.bfloat16), 'ep', axis=1, tiled=True)  17.3 us
    all_to_all x1, waiting for transfers between devices, per_device(): lax.all_to_all(expert_rows, 'ep', split_axis=1, concat_axis=0, tiled=True)  6.42 us
    all_to_all x1, starting transfers between devices, per_device(): lax.all_to_all(send_query, 'ep', split_axis=0, concat_axis=0, tiled=True)  5.98 us
    dot_general x4, matrix products, outgoing(): jnp.dot(picker, projected, preferred_element_type=jnp.float32)  5.92 us
    all_to_all x1, waiting for transfers between devices, per_device(): lax.all_to_all(send_value, 'ep', split_axis=0, concat_axis=0, tiled=True)  5.56 us
  transfers between devices with their start and end apart: 5, of which 3 were waited for; matrix products, arithmetic and copies ran while one was open for 12% of the time, Pallas kernels for 0%

commit v1 on v0

--- a/solution.py
+++ b/solution.py
@@ -11,6 +11,12 @@
 TOP = 2
 norm_eps = 1e-06
 decay_tau = 16.0
+
+
+def swap_blocks(value, name, split, join):
+    shards = jnp.split(value, lax.axis_size(name), axis=split)
+    arrived = lax.all_to_all(jnp.stack(shards), name, 0, 0)
+    return jnp.concatenate(arrived, axis=join)
 
 
 def rms_scale(values, gain):
@@ -152,7 +158,7 @@
     expert_rows = jnp.dot(active, expert_down[0], preferred_element_type=jnp.float32).astype(
         jnp.bfloat16
     )
-    arrived = lax.all_to_all(expert_rows, "ep", split_axis=1, concat_axis=0, tiled=True)
+    arrived = swap_blocks(expert_rows, "ep", 1, 0)
     every = jnp.arange(devices, dtype=jnp.int32)
     hit_all = jnp.sum((routes[:, :, None] == every[None, None, :]).astype(jnp.int32), axis=1)
     slot_all = jnp.cumsum(hit_all, axis=0) - hit_all

time: 170 us -> 179 us (1.053)
  local copies, waits for them, and re-layouts: 7.43 us -> 16.7 us
    unnamed x21 -> x36, local copies, waits for them, and re-layouts: 3.27 us -> 11.9 us
where the time goes in v1:
time: 179 us; the launch traced here: 178 us
  blocking collectives  92.6 us (52%)
  matrix products  21.6 us (12%)
  starting transfers between devices  19.8 us (11%)
  waiting for transfers between devices  17.5 us (10%)
  local copies, waits for them, and re-layouts  16.7 us (9%)
  other arithmetic  8.69 us (5%)
    psum x1, blocking collectives, per_device(): total = lax.psum(jnp.sum(floats * floats, axis=1), 'ep')  29.8 us
    all_gather x1, blocking collectives, per_device(): rows = lax.all_gather(residual, 'ep', axis=1, tiled=True)  23.7 us
    all_gather x1, blocking collectives, per_device(): lax.all_gather(mixed, 'ep', axis=0, tiled=True)  21.8 us
    all_gather x1, blocking collectives, per_device(): lax.all_gather(scaled.astype(jnp.bfloat16), 'ep', axis=1, tiled=True)  17.3 us
    unnamed x36, local copies, waits for them, and re-layouts  11.9 us
    all_to_all x1, waiting for transfers between devices, swap_blocks(): arrived = lax.all_to_all(jnp.stack(shards), name, 0, 0)  6.42 us
    all_to_all x1, starting transfers between devices, per_device(): lax.all_to_all(send_query, 'ep', split_axis=0, concat_axis=0, tiled=True)  5.98 us
    dot_general x4, matrix products, outgoing(): jnp.dot(picker, projected, preferred_element_type=jnp.float32)  5.92 us
  transfers between devices with their start and end apart: 5, of which 3 were waited for; matrix products, arithmetic and copies ran while one was open for 12% of the time, Pallas kernels for 0%

profile of v1, /device:TPU:0, one launch (start us, length us, event | category | flops | bytes accessed | tf_op | source)
XLA Modules:
  0.0 177.8 jit_solution(13739551876777802191)
XLA Ops:
  0.7 23.7 %all_gather.9 = bf16[8,4096]{1,0:T(8,128)(2,1)S(1)} all-gather(bf16[8,256]{1,0:T(8,128)(2,1)} %param.29), channel_id=1, replica_groups=mesh['grp'=2,'ep'=16] {'ep'}, dimensions={1}, use_global_device_ids=true | all-gather | bytes 69632 | tf_op jit(solution)/shard_map/all_gather | solution.py:71
  24.6 0.7 convert_element_type.145
  25.3 1.6 fusion.14
  26.9 0.6 copy.61
  27.5 3.4 %all-to-all-start.1 = ((bf16[16,1,128]{2,1,0:T(2,128)(2,1)}), bf16[16,1,128]{2,1,0:T(2,128)(2,1)S(1)}, u32[]{:S(2)}, u32[]{:S(2)}) async-start(bf16[16,1,128]{2,1,0:T(2,128)(2,1)} %copy.61), calls=%async_computation.1 | async-start | bytes 16384 | tf_op jit(solution)/shard_map/all_to_all | solution.py:93
  31.0 0.7 fusion.69
  31.7 0.7 fusion.72
  32.4 0.8 convert_reduce_fusion
  33.6 1.1 fusion.87
  34.8 1.0 convolution_add_fusion
  35.8 1.6 fusion.13
  37.4 2.1 %fusion.6 = bf16[16,1,256]{2,0,1:T(8,128)(2,1)S(1)} fusion(bf16[4096,256]{1,0:T(8,128)(2,1)} %param.35, s32[16]{0:T(128)S(1)} %and_select_fusion.1, pred[16]{0:T(512)(128)(4,1)S(1)} %broadcast_compare_fusion.2, bf16[8,4096]{1,0:T(8,128)(2,1)S(1)} %all_gather.9, f32[4096]{0:T(1024)S(1)} %convert_element_type.145, f32[8]{0:T(128)S(1)} %add_rsqrt_fusion.2), kind=kOutput, calls=%fused_computation.16 | convolution fusion | flops 16980224 | bytes 2187376 | tf_op jit(solution)/shard_map/dot_general | solution.py:84
  39.9 0.8 dynamic-slice_convert_fusion
  41.3 0.6 reduce.5
  43.2 0.6 reduce.4
  44.5 6.0 %all-to-all-start = ((bf16[16,1,128]{2,1,0:T(2,128)(2,1)}), bf16[16,1,128]{2,1,0:T(2,128)(2,1)S(1)}, u32[]{:S(2)}, u32[]{:S(2)}) async-start(bf16[16,1,128]{2,1,0:T(2,128)(2,1)} %copy.59), calls=%async_computation | async-start | bytes 16384 | tf_op jit(solution)/shard_map/all_to_all | solution.py:92
  51.3 5.5 %all-to-all-done = bf16[16,1,128]{2,1,0:T(2,128)(2,1)S(1)} async-done(((bf16[16,1,128]{2,1,0:T(2,128)(2,1)}), bf16[16,1,128]{2,1,0:T(2,128)(2,1)S(1)}, u32[]{:S(2)}, u32[]{:S(2)}) %all-to-all-start) | async-done | bytes 4128 | tf_op jit(solution)/shard_map/all_to_all | solution.py:92
  56.8 3.4 %all-to-all-start.2 = ((bf16[16,2,128]{2,1,0:T(2,128)(2,1)}), bf16[16,2,128]{2,1,0:T(2,128)(2,1)S(1)}, u32[]{:S(2)}, u32[]{:S(2)}) async-start(bf16[16,2,128]{2,1,0:T(2,128)(2,1)} %reshape.328), calls=%async_computation.2 | async-start | bytes 16384 | tf_op jit(solution)/shard_map/all_to_all | solution.py:94
  61.1 5.6 %all-to-all-done.2 = bf16[16,2,128]{2,1,0:T(2,128)(2,1)S(1)} async-done(((bf16[16,2,128]{2,1,0:T(2,128)(2,1)}), bf16[16,2,128]{2,1,0:T(2,128)(2,1)S(1)}, u32[]{:S(2)}, u32[]{:S(2)}) %all-to-all-start.2) | async-done | bytes 8224 | tf_op jit(solution)/shard_map/all_to_all | solution.py:94
  66.6 3.5 %all-to-all-start.3 = ((bf16[16,2,128]{2,1,0:T(2,128)(2,1)}), bf16[16,2,128]{2,1,0:T(2,128)(2,1)S(1)}, u32[]{:S(2)}, u32[]{:S(2)}) async-start(bf16[16,2,128]{2,1,0:T(2,128)(2,1)} %reshape.326), calls=%async_computation.3 | async-start | bytes 16384 | tf_op jit(solution)/shard_map/all_to_all | solution.py:95
  71.0 2.7 %multiply_add_fusion = f32[2,512,1024]{2,1,0:T(8,128)S(1)} fusion(f32[2,512,1024]{2,1,0:T(8,128)} %param.30, f32[2,1024]{1,0:T(2,128)S(1)} %bitcast.182, f32[2,512]{1,0:T(2,128)S(1)} %bitcast.184, f32[2,512]{1,0:T(2,128)S(1)} %fusion.43), kind=kLoop, calls=%fused_computation.11 | loop fusion | flops 3145728 | bytes 8404992 | tf_op jit(solution)/shard_map/add | solution.py:122
  73.8 2.0 %copy-done.1 = f32[2,512,1024]{2,1,0:T(8,128)} copy-done((f32[2,512,1024]{2,1,0:T(8,128)}, f32[2,512,1024]{2,1,0:T(8,128)S(1)}, u32[]{:S(2)}) %copy-start.1) | copy-done | bytes 4194328
  75.8 2.1 %fusion.91 = f32[2,1,1024]{2,1,0:T(1,128)S(1)} fusion(f32[2,512,1]{1,2,0:T(1,128)S(1)} %bitcast.183, f32[2,512,1024]{2,1,0:T(8,128)S(1)} %multiply_add_fusion), kind=kOutput, calls=%fused_computation.173 | convolution fusion | flops 12582912 | bytes 4206592 | tf_op jit(solution)/shard_map/pk,pkv->pv/dot_general | solution.py:125
  78.9 21.8 %all-gather = bf16[16,2,1024]{2,1,0:T(2,128)(2,1)S(1)} all-gather(bf16[1,2,1024]{2,1,0:T(2,128)(2,1)S(1)} %fusion.59), channel_id=1, replica_groups=mesh['grp'=2,'ep'=16] {'ep'}, dimensions={0}, use_global_device_ids=true | all-gather | bytes 69632 | tf_op jit(solution)/shard_map/all_gather | solution.py:134
  100.8 2.1 %multiply_reduce_fusion = (f32[8]{0:T(128)S(1)}, f32[8,256]{1,0:T(8,128)S(1)}) fusion(bf16[8,4096]{1,0:T(8,128)(2,1)S(1)} %reshape.282, bf16[4096,256]{1,0:T(8,128)(2,1)} %param.40, bf16[8,256]{1,0:T(8,128)(2,1)S(1)} %copy-done.2), kind=kOutput, calls=%fused_computation.73 | convolution fusion | flops 16793592 | bytes 2175008 | tf_op jit(solution)/shard_map/dot_general | solution.py:135
  102.9 29.8 %psum.7 = f32[8]{0:T(128)S(1)} all-reduce(f32[8]{0:T(128)S(1)} %get-tuple-element.2), channel_id=1, replica_groups=mesh['grp'=2,'ep'=16] {'ep'}, use_global_device_ids=true, to_apply=%region_7.8 | all-reduce | flops 8 | bytes 64 | tf_op jit(solution)/shard_map/psum | solution.py:138
  132.8 17.3 %all_gather.11 = bf16[8,4096]{1,0:T(8,128)(2,1)S(1)} all-gather(bf16[8,256]{1,0:T(8,128)(2,1)S(1)} %multiply_convert_fusion), channel_id=1, replica_groups=mesh['grp'=2,'ep'=16] {'ep'}, dimensions={1}, use_global_device_ids=true | all-gather | bytes 69632 | tf_op jit(solution)/shard_map/all_gather | solution.py:141
  150.2 2.8 %fusion.3 = f32[2,512]{1,0:T(2,128)S(1)} fusion(bf16[2,4096]{1,0:T(2,128)(2,1)S(1)} %convolution_convert_fusion.1, bf16[1,4096,512]{2,1,0:T(8,128)(2,1)} %param.45), kind=kOutput, calls=%fused_computation.9 | convolution fusion | flops 8388608 | bytes 4214784 | tf_op jit(solution)/shard_map/dot_general | solution.py:155
  153.1 4.8 %convolution_convert_fusion = bf16[2,4096]{1,0:T(2,128)(2,1)S(1)} fusion(bf16[1,512,4096]{2,1,0:T(8,128)(2,1)} %param.47, bf16[2,4096]{1,0:T(2,128)(2,1)S(1)} %convolution_convert_fusion.1, bf16[1,4096,512]{2,1,0:T(8,128)(2,1)} %param.46, f32[2,512]{1,0:T(2,128)S(1)} %fusion.3, f32[2]{0:T(128)S(1)} %convolution_bitcast_fusion.5), kind=kOutput, calls=%fused_computation.4 | convolution fusion | flops 16792576 | bytes 8425480 | tf_op jit(solution)/shard_map/dot_general | solution.py:158
  167.1 3.5 %all-to-all-start.4 = ((bf16[16,2,256]{2,1,0:T(2,128)(2,1)}), bf16[16,2,256]{2,1,0:T(2,128)(2,1)S(1)}, u32[]{:S(2)}, u32[]{:S(2)}) async-start(bf16[16,2,256]{2,1,0:T(2,128)(2,1)} %constant_dynamic-update-slice_fusion), calls=%async_computation.4 | async-start | bytes 32768 | tf_op jit(solution)/shard_map/all_to_all | solution.py:18
  170.6 6.4 %all-to-all-done.4 = bf16[16,2,256]{2,1,0:T(2,128)(2,1)S(1)} async-done(((bf16[16,2,256]{2,1,0:T(2,128)(2,1)}), bf16[16,2,256]{2,1,0:T(2,128)(2,1)S(1)}, u32[]{:S(2)}, u32[]{:S(2)}) %all-to-all-start.4) | async-done | bytes 16416 | tf_op jit(solution)/shard_map/all_to_all | solution.py:18
  177.0 0.8 fusion.8
  (92 shorter events, 16.7 us)
Async XLA Ops:
  0.6 32.5 %copy-start = (bf16[4096,256]{1,0:T(8,128)(2,1)S(1)}, bf16[4096,256]{1,0:T(8,128)(2,1)}, u32[]{:S(2)}) copy-start(bf16[4096,256]{1,0:T(8,128)(2,1)} %param.34) | copy-start | bytes 6291460
  0.6 40.0 %copy-start.3 = (s32[8,2]{0,1:T(2,128)S(1)}, s32[8,2]{0,1:T(2,128)}, u32[]{:S(2)}) copy-start(s32[8,2]{0,1:T(2,128)} %param.42) | copy-start | bytes 196
  0.7 39.1 %copy-start.4 = (f32[8,4]{0,1:T(4,128)S(1)}, f32[8,4]{0,1:T(4,128)}, u32[]{:S(2)}) copy-start(f32[8,4]{0,1:T(4,128)} %param.43) | copy-start | bytes 388
  0.7 39.1 %copy-start.6 = (f32[8,2]{0,1:T(2,128)S(1)}, f32[8,2]{0,1:T(2,128)}, u32[]{:S(2)}) copy-start(f32[8,2]{0,1:T(2,128)} %param.44) | copy-start | bytes 196
  0.7 43.8 %copy-start.5 = (bf16[1024]{0:T(1024)(128)(2,1)S(1)}, bf16[1024]{0:T(1024)(128)(2,1)}, u32[]{:S(2)}) copy-start(bf16[1024]{0:T(1024)(128)(2,1)} %param.39) | copy-start | bytes 6148
  27.5 16.9 %all-to-all-start.1 = ((bf16[16,1,128]{2,1,0:T(2,128)(2,1)}), bf16[16,1,128]{2,1,0:T(2,128)(2,1)S(1)}, u32[]{:S(2)}, u32[]{:S(2)}) async-start(bf16[16,1,128]{2,1,0:T(2,128)(2,1)} %copy.61), calls=%async_computation.1 | async-start | bytes 16384 | tf_op jit(solution)/shard_map/all_to_all | solution.py:93
  44.5 12.3 %all-to-all-start = ((bf16[16,1,128]{2,1,0:T(2,128)(2,1)}), bf16[16,1,128]{2,1,0:T(2,128)(2,1)S(1)}, u32[]{:S(2)}, u32[]{:S(2)}) async-start(bf16[16,1,128]{2,1,0:T(2,128)(2,1)} %copy.59), calls=%async_computation | async-start | bytes 16384 | tf_op jit(solution)/shard_map/all_to_all | solution.py:92
  56.8 9.8 %all-to-all-start.2 = ((bf16[16,2,128]{2,1,0:T(2,128)(2,1)}), bf16[16,2,128]{2,1,0:T(2,128)(2,1)S(1)}, u32[]{:S(2)}, u32[]{:S(2)}) async-start(bf16[16,2,128]{2,1,0:T(2,128)(2,1)} %reshape.328), calls=%async_computation.2 | async-start | bytes 16384 | tf_op jit(solution)/shard_map/all_to_all | solution.py:94
  66.6 11.3 %all-to-all-start.3 = ((bf16[16,2,128]{2,1,0:T(2,128)(2,1)}), bf16[16,2,128]{2,1,0:T(2,128)(2,1)S(1)}, u32[]{:S(2)}, u32[]{:S(2)}) async-start(bf16[16,2,128]{2,1,0:T(2,128)(2,1)} %reshape.326), calls=%async_computation.3 | async-start | bytes 16384 | tf_op jit(solution)/shard_map/all_to_all | solution.py:95
  73.7 2.0 %copy-start.1 = (f32[2,512,1024]{2,1,0:T(8,128)}, f32[2,512,1024]{2,1,0:T(8,128)S(1)}, u32[]{:S(2)}) copy-start(f32[2,512,1024]{2,1,0:T(8,128)S(1)} %multiply_add_fusion) | copy-start | bytes 12582916
  73.8 27.0 %copy-start.2 = (bf16[8,256]{1,0:T(8,128)(2,1)S(1)}, bf16[8,256]{1,0:T(8,128)(2,1)}, u32[]{:S(2)}) copy-start(bf16[8,256]{1,0:T(8,128)(2,1)} %param.29) | copy-start | bytes 12292
  167.1 10.0 %all-to-all-start.4 = ((bf16[16,2,256]{2,1,0:T(2,128)(2,1)}), bf16[16,2,256]{2,1,0:T(2,128)(2,1)S(1)}, u32[]{:S(2)}, u32[]{:S(2)}) async-start(bf16[16,2,256]{2,1,0:T(2,128)(2,1)} %constant_dynamic-update-slice_fusion), calls=%async_computation.4 | async-start | bytes 32768 | tf_op jit(solution)/shard_map/all_to_all | solution.py:18
